TPU v7x, 32 devices: a whole 2x2x4 slice. The times are simulated.
32 devices in a mesh: sp: 16 (over z, y, x), tp: 2 (over core).
Axes of the slice: x: 2, y: 2, z: 4, core: 2. Of those that a mesh axis runs over, the one named last changes fastest.
Arguments:
- queries: bfloat16 [4096, 512], P('sp', 'tp'), may hold values from -6 to 6
- keys: bfloat16 [4096, 512], P('sp', 'tp'), may hold values from -6 to 6
- values: bfloat16 [4096, 512], P('sp', 'tp'), may hold values from -6 to 6
- gains: float32 [2, 128], replicated, may hold values from 0.1 to 1.9
- bias_table: float32 [192, 4], P(None, 'tp'), may hold values from -6 to 270
- d_out: bfloat16 [4096, 512], P('sp', 'tp'), may hold values from -32 to 32
Outputs:
- d_queries: bfloat16 [4096, 512], P('sp', 'tp')
- d_keys: bfloat16 [4096, 512], P('sp', 'tp')
- d_values: bfloat16 [4096, 512], P('sp', 'tp')
- d_table: float32 [192, 4], P(None, 'tp')
- d_gains: float32 [2, 128], replicated
All inputs are finite; a program needn't handle non-finite values.
Results may differ from a plain program's by a relative error of at most 0.008.
Values may be sent and summed in bfloat16 or wider, within the bound.
No kernel may reach another device: no remote copies, remote signals or barrier semaphores. Data moves between devices by JAX's collectives and lax.ppermute only.
A program may use at most 64 MiB of HBM per device.

v0:
```python
import jax
import jax.numpy as jnp
from jax import lax
from jax.sharding import PartitionSpec as P

HEADS = 4
HEAD_DIM = 128
SEG = 64
LEFT = 4
MAX_REL = 128


EPSILON = 1e-06


def shifted(block, axis, distance):
    devices = range(lax.axis_size(axis))
    route = [(i - distance, i) for i in devices if i - distance in devices]
    return lax.ppermute(block, axis, route)


def norm_rows(row_block, gain_vec):
    row_count = row_block.shape[0]
    widened = row_block.astype(jnp.float32).reshape(row_count, -1, HEAD_DIM)
    inv_rms = lax.rsqrt(jnp.mean(widened * widened, axis=-1, keepdims=True) + EPSILON)
    unit_part = widened * inv_rms
    return ((unit_part * gain_vec).astype(jnp.bfloat16).reshape(row_count, -1), unit_part, inv_rms)


def norm_back(d_normed, unit_part, inv_rms, gain_vec):
    d_unit = d_normed * gain_vec
    d_rows = inv_rms * (d_unit - unit_part * jnp.mean(d_unit * unit_part, axis=-1, keepdims=True))
    return (
        d_rows.reshape(unit_part.shape[0], -1).astype(jnp.bfloat16),
        jnp.sum(d_normed * unit_part, axis=(0, 1)),
    )


def build_bias(table_heads):
    head_count, entries = table_heads.shape
    last_entry = table_heads[:, entries - 1 :]
    padded = jnp.concatenate(
        [table_heads, jnp.broadcast_to(last_entry, (head_count, SEG - 1))], axis=1
    )
    length = entries + SEG - 1
    repeated = jnp.tile(padded, (1, SEG + 1))[:, : SEG * (length + 1)]
    hankel = repeated.reshape(head_count, SEG, length + 1)[:, :, :entries]
    near_part = hankel[:, :, ::-1]
    far_part = jnp.broadcast_to(last_entry[:, :, None], (head_count, SEG, LEFT * SEG - MAX_REL))
    return jnp.concatenate([far_part, near_part], axis=2)


def table_grad(d_band):
    head_count = d_band.shape[0]
    far_width = LEFT * SEG - MAX_REL
    far_total = jnp.sum(d_band[:, :, :far_width], axis=(1, 2))
    flipped = d_band[:, :, far_width:][:, :, ::-1]
    entries = flipped.shape[2]
    width = entries + SEG
    padded = jnp.pad(flipped, ((0, 0), (0, 0), (0, SEG)))
    skewed = padded.reshape(head_count, SEG * width)[:, : SEG * (width - 1)].reshape(
        head_count, SEG, width - 1
    )
    columns = jnp.sum(skewed, axis=1)
    tail_sum = jnp.sum(columns[:, entries - 1 :], axis=1) + far_total
    return jnp.concatenate([columns[:, : entries - 1], tail_sum[:, None]], axis=1).T


def band_of(rows_ext, seg_count):
    feature_count = rows_ext.shape[1]
    segments = rows_ext.reshape(LEFT + seg_count, SEG, feature_count)
    stacked = jnp.stack(
        [segments[offset : offset + seg_count] for offset in range(LEFT + 1)], axis=1
    )
    return stacked.reshape(seg_count, (LEFT + 1) * SEG, feature_count)


def unband(grad_band, seg_count):
    pieces = grad_band.reshape(seg_count, LEFT + 1, SEG, -1)
    summed = jnp.zeros((LEFT + seg_count, SEG, pieces.shape[3]), jnp.float32)
    for offset in range(LEFT + 1):
        summed = summed + jnp.pad(pieces[:, offset], ((offset, LEFT - offset), (0, 0), (0, 0)))
    return summed.reshape((LEFT + seg_count) * SEG, -1)


def band_grads(q_norm, d_out, k_ext, v_ext, bias_tiles, key_valid):
    seg_count = q_norm.shape[0] // SEG
    head_count = bias_tiles.shape[0]
    factor = HEAD_DIM ** (-0.5)
    q_seg = q_norm.reshape(seg_count, SEG, head_count, HEAD_DIM)
    do_seg = d_out.reshape(seg_count, SEG, head_count, HEAD_DIM)
    k_band = band_of(k_ext, seg_count).reshape(seg_count, -1, head_count, HEAD_DIM)
    v_band = band_of(v_ext, seg_count).reshape(seg_count, -1, head_count, HEAD_DIM)
    scores = (
        jnp.einsum("cihd,cjhd->chij", q_seg, k_band, preferred_element_type=jnp.float32) * factor
        + bias_tiles[None]
    )
    scores = jnp.where(key_valid, scores, -jnp.inf)
    row_max = jnp.max(scores, axis=-1, keepdims=True)
    log_total = row_max + jnp.log(jnp.sum(jnp.exp(scores - row_max), axis=-1, keepdims=True))
    prob = jnp.exp(scores - log_total)
    d_prob = jnp.einsum("cihd,cjhd->chij", do_seg, v_band, preferred_element_type=jnp.float32)
    row_delta = jnp.sum(prob * d_prob, axis=-1, keepdims=True)
    d_score = prob * (d_prob - row_delta)
    prob_low = prob.astype(jnp.bfloat16)
    d_low = d_score.astype(jnp.bfloat16)
    grad_v = jnp.einsum("chij,cihd->cjhd", prob_low, do_seg, preferred_element_type=jnp.float32)
    grad_k = (
        jnp.einsum("chij,cihd->cjhd", d_low, q_seg, preferred_element_type=jnp.float32) * factor
    )
    grad_q = (
        jnp.einsum("chij,cjhd->cihd", d_low, k_band, preferred_element_type=jnp.float32) * factor
    )
    grad_q = grad_q.reshape(seg_count * SEG, head_count, HEAD_DIM)
    return (
        grad_q,
        unband(grad_k, seg_count),
        unband(grad_v, seg_count),
        jnp.sum(d_score, axis=0),
        log_total,
        row_delta,
    )


def local(queries, keys, values, gains, bias_table, d_out):
    row_count, feature_count = queries.shape
    head_count = feature_count // HEAD_DIM
    tail_rows = LEFT * SEG
    seg_count = row_count // SEG
    device_slot = lax.axis_index("sp")
    q_norm, q_unit, q_rms = norm_rows(queries, gains[0])
    k_norm, k_unit, k_rms = norm_rows(keys, gains[1])
    earlier_k, earlier_v = shifted((k_norm, values), "sp", 1)
    k_ext = jnp.concatenate([earlier_k, k_norm])
    v_ext = jnp.concatenate([earlier_v, values])
    bias_tiles = build_bias(bias_table.T)
    band_seg = jnp.arange((LEFT + 1) * SEG, dtype=jnp.int32) // SEG
    key_seg = (
        device_slot * seg_count
        + jnp.arange(seg_count, dtype=jnp.int32)[:, None]
        - LEFT
        + band_seg[None, :]
    )
    key_valid = (key_seg >= 0)[:, None, None, :]
    d_qn, dk_ext, dv_ext, d_band, log_total, row_delta = band_grads(
        q_norm, d_out, k_ext, v_ext, bias_tiles, key_valid
    )
    dk_own = dk_ext[tail_rows:]
    dv_own = dv_ext[tail_rows:]
    back_k, back_v = (
        shifted(dk_ext[:tail_rows].astype(jnp.bfloat16), "sp", -1).astype(jnp.float32),
        shifted(dv_ext[:tail_rows].astype(jnp.bfloat16), "sp", -1).astype(jnp.float32),
    )
    dk_total = dk_own + back_k
    dv_total = dv_own + back_v
    d_queries, gain_q = norm_back(d_qn, q_unit, q_rms, gains[0])
    d_keys, gain_k = norm_back(
        dk_total.reshape(row_count, head_count, HEAD_DIM), k_unit, k_rms, gains[1]
    )
    d_values = dv_total.astype(jnp.bfloat16)
    table_part = table_grad(d_band)
    gain_part = jnp.stack([gain_q, gain_k])
    head_start = lax.axis_index("tp") * head_count
    whole_table = jnp.zeros((table_part.shape[0], HEADS), jnp.float32)
    whole_table = lax.dynamic_update_slice(whole_table, table_part, (0, head_start))
    whole_table, d_gains = lax.psum((whole_table, gain_part), ("sp", "tp"))
    d_table = lax.dynamic_slice(whole_table, (0, head_start), (table_part.shape[0], head_count))
    return (d_queries, d_keys, d_values, d_table, d_gains)


def solution(mesh):
    in_specs = (P("sp", "tp"), P("sp", "tp"), P("sp", "tp"), P(), P(None, "tp"), P("sp", "tp"))
    out_specs = (P("sp", "tp"), P("sp", "tp"), P("sp", "tp"), P(None, "tp"), P())
    return jax.shard_map(local, mesh=mesh, in_specs=in_specs, out_specs=out_specs, check_vma=False)
```

profile of v0, /device:TPU:0, one launch (start us, length us, event | category | flops | bytes accessed | tf_op | source)
XLA Modules:
  0.0 89.2 jit_solution(15028463955493800974)
XLA Ops:
  0.7 5.0 %collective-permute-start.1 = (bf16[256,256]{1,0:T(8,128)(2,1)}, bf16[256,256]{1,0:T(8,128)(2,1)S(1)}, u32[]{:S(2)}, u32[]{:S(2)}) collective-permute-start(bf16[256,256]{1,0:T(8,128)(2,1)} %param.8), channel_id=1, source_target_pairs={{0,2},{2,4},{4,6},{6,8},{8,10},{10,12},{12,14},{14,16},{16,18},{18... | collective-permute-start | bytes 393224 | tf_op jit(solution)/shard_map/ppermute | solution.py:19
  5.7 0.8 slice_bitcast_fusion.10
  6.5 1.0 %reshape.206 = f32[256,2,128]{2,1,0:T(2,128)S(1)} reshape(bf16[256,256]{1,0:T(8,128)(2,1)} %param.7) | data formatting | bytes 393216 | tf_op jit(solution)/shard_map/reshape | solution.py:24
  7.5 0.3 multiply_reduce_fusion.4
  7.9 0.3 mul.196
  8.3 3.4 %collective-permute-start = (bf16[256,256]{1,0:T(8,128)(2,1)S(1)}, bf16[256,256]{1,0:T(8,128)(2,1)S(1)}, u32[]{:S(2)}, u32[]{:S(2)}) collective-permute-start(bf16[256,256]{1,0:T(8,128)(2,1)S(1)} %multiply_convert_fusion.1), channel_id=1, source_target_pairs={{0,2},{2,4},{4,6},{6,8},{8,10},{10,12},{12,14},{14,16},{16,18},{18... | collective-permute-start | bytes 393224 | tf_op jit(solution)/shard_map/ppermute | solution.py:19
  11.7 0.5 broadcast_multiply_fusion.1
  12.2 0.2 slice_reduce_fusion.2
  12.4 0.6 broadcast_bitcast_fusion
  13.0 0.1 mul.192
  13.2 0.3 reduce_sum.115
  13.6 0.1 add_compare_fusion
  13.7 0.1 pad_maximum_fusion.2
  13.8 0.1 reshape.207
  14.0 0.3 tile.10
  14.3 0.2 reverse
  14.5 0.1 slice.208
  14.6 0.1 copy.149
  14.7 0.1 broadcast_in_dim.22
  14.9 0.1 copy-done.14
  15.1 0.2 reshape_reshape.7
  15.4 0.2 reshape_reshape.8
  15.6 0.5 fusion.29
  16.1 0.3 exponential_reduce_fusion
  16.4 0.4 multiply_reduce_fusion
  16.8 0.3 fusion.18
  17.1 0.6 slice_reduce_fusion
  17.7 0.7 slice.172
  18.4 0.6 convolution_bitcast_fusion
  19.0 0.5 fusion
  19.5 0.2 copy-done.23
  19.6 1.5 %multiply_reduce_fusion.2 = (f32[128]{0:T(128)}, f32[4,64,2]{1,2,0:T(2,128)S(1)}, f32[4,2,128,64]{2,3,1,0:T(8,128)}) fusion(f32[4,64,2,128]{3,2,1,0:T(2,128)S(1)} %copy-done.1, f32[4,64,2]{1,2,0:T(2,128)S(1)} %copy.149, f32[128]{0:T(128)S(1)} %copy-done.23, bf16[4,2,64,320]{3,2,1,0:T(8,128)(2,1)S(1)} %get-tuple-element.12, ...), kind=kOutput, calls=%fused_computation.53 | convolution fusion | flops 42401152 | bytes 1512448 | tf_op jit(solution)/shard_map/chij,cjhd->cihd/dot_general | solution.py:112
  21.1 1.0 %reverse.1 = f32[2,64,256]{2,1,0:T(8,128)S(1)} reverse(f32[2,64,256]{2,1,0:T(8,128)} %bitcast.190), dimensions={2} | reverse | bytes 262144
  22.1 0.1 slice.209
  22.3 0.1 copy.192
  22.4 0.2 reshape.215
  22.6 0.8 slice_reduce_fusion.1
  23.4 0.1 copy.177
  23.6 0.9 %copy.160 = f32[4,64,2,128]{3,2,1,0:T(2,128)} copy(f32[4,64,2,128]{3,1,2,0:T(8,128)S(1)} %multiply_bitcast_fusion) | data formatting | bytes 524288 | tf_op jit(solution)/shard_map/mul | solution.py:112
  24.5 2.1 %copy.171 = f32[4,320,2,128]{3,2,1,0:T(2,128)} copy(f32[4,320,2,128]{3,1,2,0:T(8,128)S(1)} %convolution_bitcast_fusion) | data formatting | bytes 2621440 | tf_op jit(solution)/shard_map/chij,cihd->cjhd/transpose | solution.py:107
  26.5 2.3 %reshape.213 = f32[4,5,64,256]{3,2,1,0:T(8,128)S(1)} reshape(f32[4,320,2,128]{3,2,1,0:T(2,128)} %copy.171) | data formatting | bytes 2621440 | tf_op jit(solution)/shard_map/reshape | solution.py:79
  28.9 0.1 slice_bitcast_fusion.4
  29.0 0.1 pad_add_fusion
  29.1 0.7 slice.210
  29.8 1.3 %collective-permute-start.3 = (bf16[256,256]{1,0:T(8,128)(2,1)}, bf16[256,256]{1,0:T(8,128)(2,1)}, u32[]{:S(2)}, u32[]{:S(2)}) collective-permute-start(bf16[256,256]{1,0:T(8,128)(2,1)} %bitcast.44), channel_id=1, source_target_pairs={{2,0},{4,2},{6,4},{8,6},{10,8},{12,10},{14,12},{16,14},{18,16},{20... | collective-permute-start | bytes 393224 | tf_op jit(solution)/shard_map/ppermute | solution.py:19
  31.1 1.0 %copy.163 = f32[4,320,2,128]{3,2,1,0:T(2,128)S(1)} copy(f32[4,320,2,128]{3,1,2,0:T(8,128)S(1)} %fusion) | data formatting | bytes 2621440 | tf_op jit(solution)/shard_map/mul | solution.py:109
  32.1 1.0 %reshape.211 = f32[4,5,64,256]{3,2,1,0:T(8,128)S(1)} reshape(f32[4,320,2,128]{3,2,1,0:T(2,128)S(1)} %copy.163) | data formatting | bytes 2621440 | tf_op jit(solution)/shard_map/reshape | solution.py:79
  33.2 0.1 slice_bitcast_fusion.9
  33.3 0.1 pad_add_fusion.1
  33.5 1.6 %collective-permute-start.2 = (bf16[256,256]{1,0:T(8,128)(2,1)S(1)}, bf16[256,256]{1,0:T(8,128)(2,1)S(1)}, u32[]{:S(2)}, u32[]{:S(2)}) collective-permute-start(bf16[256,256]{1,0:T(8,128)(2,1)S(1)} %bitcast.197), channel_id=1, source_target_pairs={{2,0},{4,2},{6,4},{8,6},{10,8},{12,10},{14,12},{16,14},{18,16},{20... | collective-permute-start | bytes 393224 | tf_op jit(solution)/shard_map/ppermute | solution.py:19
  35.1 0.3 mul.193
  35.4 0.3 mul.228
  35.8 0.7 fusion.15
  36.6 0.1 copy.176
  36.7 0.1 fusion.26
  36.8 4.3 %collective-permute-done.2 = bf16[256,256]{1,0:T(8,128)(2,1)S(1)} collective-permute-done((bf16[256,256]{1,0:T(8,128)(2,1)S(1)}, bf16[256,256]{1,0:T(8,128)(2,1)S(1)}, u32[]{:S(2)}, u32[]{:S(2)}) %collective-permute-start.2) | collective-permute-done | bytes 131104 | tf_op jit(solution)/shard_map/ppermute | solution.py:19
  41.1 0.1 multiply_reduce_fusion.1
  41.2 0.1 reshape.212
  41.4 0.6 multiply_reduce_fusion.3
  42.0 0.3 mul.240
  42.4 0.7 fusion.12
  43.1 43.9 %all-reduce.11 = (f32[192,4]{0,1:T(4,128)S(1)}, f32[2,128]{1,0:T(2,128)}) all-reduce(f32[192,4]{0,1:T(4,128)S(1)} %fusion.26, f32[2,128]{1,0:T(2,128)S(1)} %pad_maximum_fusion.3), channel_id=1, replica_groups=mesh['sp'=16,'tp'=2] {'sp','tp'}, use_global_device_ids=true, to_apply=%region_11.12 | all-reduce | flops 1024 | bytes 8192 | tf_op jit(solution)/shard_map/psum | solution.py:166
  87.0 0.6 constant_dynamic-slice_fusion
  87.6 1.6 %fusion.16 = bf16[256,256]{1,0:T(8,128)(2,1)} fusion(f32[4,64,256]{2,1,0:T(8,128)S(1)} %slice-done, bf16[256,256]{1,0:T(8,128)(2,1)} %collective-permute-done.3), kind=kLoop, calls=%fused_computation.47 | loop fusion | flops 196608 | bytes 524288 | tf_op jit(solution)/shard_map/convert_element_type | solution.py:160
  (90 shorter events, 0.8 us)
Async XLA Ops:
  0.6 11.1 %copy-start.19 = (f32[2,128]{1,0:T(2,128)S(1)}, f32[2,128]{1,0:T(2,128)}, u32[]{:S(2)}) copy-start(f32[2,128]{1,0:T(2,128)} %param.9) | copy-start | bytes 3076
  0.6 7.6 %copy-start.4 = (bf16[256,256]{1,0:T(8,128)(2,1)S(1)}, bf16[256,256]{1,0:T(8,128)(2,1)}, u32[]{:S(2)}) copy-start(bf16[256,256]{1,0:T(8,128)(2,1)} %param.7) | copy-start | bytes 393220
  0.7 11.6 %copy-start.17 = (f32[192,2]{0,1:T(2,128)S(1)}, f32[192,2]{0,1:T(2,128)}, u32[]{:S(2)}) copy-start(f32[192,2]{0,1:T(2,128)} %param.10) | copy-start | bytes 4612
  0.7 12.3 %copy-start.7 = (bf16[256,256]{1,0:T(8,128)(2,1)S(1)}, bf16[256,256]{1,0:T(8,128)(2,1)}, u32[]{:S(2)}) copy-start(bf16[256,256]{1,0:T(8,128)(2,1)} %param.6) | copy-start | bytes 393220
  0.7 14.2 %collective-permute-start.1 = (bf16[256,256]{1,0:T(8,128)(2,1)}, bf16[256,256]{1,0:T(8,128)(2,1)S(1)}, u32[]{:S(2)}, u32[]{:S(2)}) collective-permute-start(bf16[256,256]{1,0:T(8,128)(2,1)} %param.8), channel_id=1, source_target_pairs={{0,2},{2,4},{4,6},{6,8},{8,10},{10,12},{12,14},{14,16},{16,18},{18... | collective-permute-start | bytes 393224 | tf_op jit(solution)/shard_map/ppermute | solution.py:19
  7.5 6.0 %copy-start.2 = (f32[256,2,128]{2,1,0:T(2,128)}, f32[256,2,128]{2,1,0:T(2,128)S(1)}, u32[]{:S(2)}) copy-start(f32[256,2,128]{2,1,0:T(2,128)S(1)} %reshape.206) | copy-start | bytes 786436
  7.9 6.0 %copy-start.11 = (f32[256,2]{1,0:T(8,128)}, f32[256,2]{1,0:T(8,128)S(1)}, u32[]{:S(2)}) copy-start(f32[256,2]{1,0:T(8,128)S(1)} %add_rsqrt_fusion) | copy-start | bytes 6148
  8.2 5.7 %copy-start.16 = (bf16[256,256]{1,0:T(8,128)(2,1)S(1)}, bf16[256,256]{1,0:T(8,128)(2,1)}, u32[]{:S(2)}) copy-start(bf16[256,256]{1,0:T(8,128)(2,1)} %param.11) | copy-start | bytes 393220
  8.3 6.7 %collective-permute-start = (bf16[256,256]{1,0:T(8,128)(2,1)S(1)}, bf16[256,256]{1,0:T(8,128)(2,1)S(1)}, u32[]{:S(2)}, u32[]{:S(2)}) collective-permute-start(bf16[256,256]{1,0:T(8,128)(2,1)S(1)} %multiply_convert_fusion.1), channel_id=1, source_target_pairs={{0,2},{2,4},{4,6},{6,8},{8,10},{10,12},{12,14},{14,16},{16,18},{18... | collective-permute-start | bytes 393224 | tf_op jit(solution)/shard_map/ppermute | solution.py:19
  13.6 1.3 %copy-start.9 = (f32[256,2]{1,0:T(8,128)}, f32[256,2]{1,0:T(8,128)S(1)}, u32[]{:S(2)}) copy-start(f32[256,2]{1,0:T(8,128)S(1)} %add_rsqrt_fusion.1) | copy-start | bytes 6148
  13.9 1.6 %copy-start = (f32[4,64,2,128]{3,2,1,0:T(2,128)}, f32[4,64,2,128]{3,2,1,0:T(2,128)S(1)}, u32[]{:S(2)}) copy-start(f32[4,64,2,128]{3,2,1,0:T(2,128)S(1)} %reshape.207) | copy-start | bytes 786436
  13.9 1.0 %copy-start.14 = (bf16[256,256]{1,0:T(8,128)(2,1)S(1)}, bf16[256,256]{1,0:T(8,128)(2,1)}, u32[]{:S(2)}) copy-start(bf16[256,256]{1,0:T(8,128)(2,1)} %param.8) | copy-start | bytes 393220
  17.1 1.9 %copy-start.1 = (f32[4,64,2,128]{3,2,1,0:T(2,128)S(1)}, f32[4,64,2,128]{3,2,1,0:T(2,128)}, u32[]{:S(2)}) copy-start(f32[4,64,2,128]{3,2,1,0:T(2,128)} %copy-done) | copy-start | bytes 786436
  19.0 0.7 copy-start.23
  21.1 2.4 %copy-start.15 = (f32[4,2,128,64]{2,3,1,0:T(8,128)S(1)}, f32[4,2,128,64]{2,3,1,0:T(8,128)}, u32[]{:S(2)}) copy-start(f32[4,2,128,64]{2,3,1,0:T(8,128)} %get-tuple-element.35) | copy-start | bytes 786436
  29.1 7.5 %copy-start.6 = (f32[8,64,256]{2,1,0:T(8,128)}, f32[8,64,256]{2,1,0:T(8,128)S(1)}, u32[]{:S(2)}) copy-start(f32[8,64,256]{2,1,0:T(8,128)S(1)} %pad_add_fusion) | copy-start | bytes 1572868
  29.8 57.8 %collective-permute-start.3 = (bf16[256,256]{1,0:T(8,128)(2,1)}, bf16[256,256]{1,0:T(8,128)(2,1)}, u32[]{:S(2)}, u32[]{:S(2)}) collective-permute-start(bf16[256,256]{1,0:T(8,128)(2,1)} %bitcast.44), channel_id=1, source_target_pairs={{2,0},{4,2},{6,4},{8,6},{10,8},{12,10},{14,12},{16,14},{18,16},{20... | collective-permute-start | bytes 393224 | tf_op jit(solution)/shard_map/ppermute | solution.py:19
  33.3 1.8 %copy-start.10 = (f32[256,2]{1,0:T(8,128)S(1)}, f32[256,2]{1,0:T(8,128)}, u32[]{:S(2)}) copy-start(f32[256,2]{1,0:T(8,128)} %copy-done.9) | copy-start | bytes 6148
  33.3 2.5 %copy-start.8 = (bf16[256,256]{1,0:T(8,128)(2,1)S(1)}, bf16[256,256]{1,0:T(8,128)(2,1)}, u32[]{:S(2)}) copy-start(bf16[256,256]{1,0:T(8,128)(2,1)} %param.6) | copy-start | bytes 393220
  33.3 2.5 %copy-start.13 = (f32[4,64,2,128]{3,2,1,0:T(2,128)S(1)}, f32[4,64,2,128]{3,2,1,0:T(2,128)}, u32[]{:S(2)}) copy-start(f32[4,64,2,128]{3,2,1,0:T(2,128)} %copy.160) | copy-start | bytes 786436
  33.3 2.5 %copy-start.18 = (f32[256]{0:T(256)S(1)}, f32[256]{0:T(256)}, u32[]{:S(2)}) copy-start(f32[256]{0:T(256)} %broadcast_bitcast_fusion) | copy-start | bytes 3076
  33.4 3.1 %copy-start.20 = (f32[2]{0:T(128)S(1)}, f32[2]{0:T(128)}, u32[]{:S(2)}) copy-start(f32[2]{0:T(128)} %slice_reduce_fusion) | copy-start | bytes 28
  33.4 3.1 %copy-start.22 = (f32[2]{0:T(128)S(1)}, f32[2]{0:T(128)}, u32[]{:S(2)}) copy-start(f32[2]{0:T(128)} %slice_reduce_fusion.1) | copy-start | bytes 28
  33.5 7.6 %collective-permute-start.2 = (bf16[256,256]{1,0:T(8,128)(2,1)S(1)}, bf16[256,256]{1,0:T(8,128)(2,1)S(1)}, u32[]{:S(2)}, u32[]{:S(2)}) collective-permute-start(bf16[256,256]{1,0:T(8,128)(2,1)S(1)} %bitcast.197), channel_id=1, source_target_pairs={{2,0},{4,2},{6,4},{8,6},{10,8},{12,10},{14,12},{16,14},{18,16},{20... | collective-permute-start | bytes 393224 | tf_op jit(solution)/shard_map/ppermute | solution.py:19
  35.4 5.7 %copy-start.5 = (bf16[256,256]{1,0:T(8,128)(2,1)S(1)}, bf16[256,256]{1,0:T(8,128)(2,1)}, u32[]{:S(2)}) copy-start(bf16[256,256]{1,0:T(8,128)(2,1)} %param.7) | copy-start | bytes 393220
  36.6 4.8 %copy-start.3 = (f32[256,2,128]{2,1,0:T(2,128)S(1)}, f32[256,2,128]{2,1,0:T(2,128)}, u32[]{:S(2)}) copy-start(f32[256,2,128]{2,1,0:T(2,128)} %copy-done.2) | copy-start | bytes 786436
  36.6 4.8 %copy-start.12 = (f32[256,2]{1,0:T(8,128)S(1)}, f32[256,2]{1,0:T(8,128)}, u32[]{:S(2)}) copy-start(f32[256,2]{1,0:T(8,128)} %copy-done.11) | copy-start | bytes 6148
  41.4 1.7 %copy-start.21 = (f32[128]{0:T(128)S(1)}, f32[128]{0:T(128)}, u32[]{:S(2)}) copy-start(f32[128]{0:T(128)} %get-tuple-element.5) | copy-start | bytes 1540
  41.4 46.2 %slice-start = ((f32[8,64,256]{2,1,0:T(8,128)}), f32[4,64,256]{2,1,0:T(8,128)S(1)}, s32[]{:S(2)}) async-start(f32[8,64,256]{2,1,0:T(8,128)} %copy-done.6), calls=%async_computation | async-start | bytes 524288 | tf_op jit(solution)/shard_map/slice | solution.py:149
where the time goes:
time: 89.6 us; the launch traced here: 89.2 us
  blocking collectives  43.9 us (49%)
  local copies, waits for them, and re-layouts  17.2 us (19%)
  starting transfers between devices  11.3 us (13%)
  other arithmetic  7.59 us (8%)
  waiting for transfers between devices  4.33 us (5%)
  matrix products  3.45 us (4%)
  between operations  1.42 us (2%)
    psum x1, blocking collectives, local(): whole_table, d_gains = lax.psum((whole_table, gain_part), ('sp', 'tp'))  43.9 us
    ppermute x4, starting transfers between devices, shifted(): return lax.ppermute(block, axis, route)  11.3 us
    ppermute x4, waiting for transfers between devices, shifted(): return lax.ppermute(block, axis, route)  4.33 us
    reshape x2, local copies, waits for them, and re-layouts, unband(): pieces = grad_band.reshape(seg_count, LEFT + 1, SEG, -1)  3.38 us
    transpose x1, local copies, waits for them, and re-layouts, band_grads(): jnp.einsum('chij,cihd->cjhd', prob_low, do_seg, preferred_element_type=jn...  2.07 us
    unnamed x64, local copies, waits for them, and re-layouts  2.01 us
  transfers between devices with their start and end apart: 4, of which 1 were waited for; matrix products, arithmetic and copies ran while one was open for 13% of the time, Pallas kernels for 0%

commit v1 on v0

v1 whole, which is shorter than its diff:
```python
import functools

import jax
import jax.numpy as jnp
from jax import lax
from jax.experimental import pallas as pl
from jax.experimental.pallas import tpu as pltpu
from jax.sharding import PartitionSpec as P

HEAD_DIM = 128
SEG = 64
LEFT = 4
MAX_REL = 128
ENTRIES = MAX_REL + SEG
EPSILON = 1e-06
FACTOR = HEAD_DIM ** (-0.5)
TAIL = LEFT * SEG

BLOCK = 2 * SEG
WINDOW = LEFT // 2 + 1
MASKED = -1e30

F32 = jnp.float32
BF16 = jnp.bfloat16


def dot(a, b, contract):
    return lax.dot_general(a, b, ((contract[:1], contract[1:]), ((), ())), preferred_element_type=F32)


def shifted(block, distance):
    devices = range(lax.axis_size("sp"))
    route = [(i - distance, i) for i in devices if i - distance in devices]
    return lax.ppermute(block, "sp", route)


def unit_rows(rows):
    rows = rows.astype(F32)
    inv_rms = lax.rsqrt(jnp.mean(rows * rows, axis=-1, keepdims=True) + EPSILON)
    return rows * inv_rms, inv_rms


def rows_back(d_normed, unit, inv_rms, gain):
    g = d_normed * gain
    return inv_rms * (g - unit * jnp.mean(g * unit, axis=-1, keepdims=True))


def lanes(shape):
    return lax.broadcasted_iota(jnp.int32, shape, len(shape) - 1)


def toeplitz(row):
    base = pltpu.roll(jnp.broadcast_to(row, (8, 2 * BLOCK)), 0, 1, stride=1, stride_axis=0)
    tiles = [base[:, :BLOCK]]
    for a in range(8, BLOCK, 8):
        tiles.append(pltpu.roll(base, a, 1)[:, :BLOCK])
    return jnp.concatenate(tiles, axis=0)


def diagonals(tile):
    width = 2 * BLOCK
    total = jnp.zeros((8, width), F32)
    empty = jnp.zeros((8, BLOCK), F32)
    for a in range(0, BLOCK, 8):
        part = jnp.concatenate([tile[a : a + 8], empty], axis=1)
        total = total + (pltpu.roll(part, width - a, 1) if a else part)
    out = total[:1]
    for s in range(1, 8):
        out = out + pltpu.roll(total, width - s, 1)[s : s + 1]
    return out


def bias_blocks(table):
    width = 2 * BLOCK
    last = table[:, ENTRIES - 1 :]
    lane = lanes((1, width))
    wide = jnp.concatenate([table, jnp.zeros((1, width - ENTRIES), F32)], axis=1)
    far = jnp.broadcast_to(last, (BLOCK, BLOCK))
    middle = toeplitz(jnp.where(lane < BLOCK, last, pltpu.roll(wide, width - (ENTRIES - 1), 1)))
    near = toeplitz(pltpu.roll(wide, width - (SEG - 1), 1))
    key = lax.broadcasted_iota(jnp.int32, (BLOCK, BLOCK), 0)
    query = lax.broadcasted_iota(jnp.int32, (BLOCK, BLOCK), 1)
    far = jnp.where((key < SEG) & (query >= SEG), MASKED, far)
    near = jnp.where((key >= SEG) & (query < SEG), MASKED, near)
    return [far, middle, near]


def table_row(far, middle, near):
    width = 2 * BLOCK
    lane = lanes((1, width))
    mid = diagonals(middle)
    last = jnp.sum(far) + jnp.sum(jnp.where(lane < BLOCK, mid, 0.0))
    mid = jnp.where(lane < BLOCK, 0.0, mid)
    row = pltpu.roll(diagonals(near), SEG - 1, 1) + pltpu.roll(mid, ENTRIES - 1, 1)
    return row + jnp.where(lane == ENTRIES - 1, last, 0.0)


def band_kernel(
    q_ref, k_ref, v_ref, do_ref, pk_ref, pv_ref, gains_ref, table_ref,
    dq_ref, back_ref, own_ref, parts_ref,
):
    rows, features = q_ref.shape
    heads = features // HEAD_DIM
    blocks = rows // BLOCK
    first = lax.axis_index("sp") == 0
    gain_q = gains_ref[0:1]
    gain_k = gains_ref[1:2]
    pieces = []
    d_gain_q = jnp.zeros((1, HEAD_DIM), F32)
    d_gain_k = jnp.zeros((1, HEAD_DIM), F32)
    for h in range(heads):
        cols = slice(h * HEAD_DIM, (h + 1) * HEAD_DIM)
        q_unit, q_rms = unit_rows(q_ref[:, cols])
        q_norm = (q_unit * gain_q).astype(BF16)
        k_unit, _ = unit_rows(jnp.concatenate([pk_ref[:, cols], k_ref[:, cols]], axis=0))
        k_norm = (k_unit * gain_k).astype(BF16)
        v_ext = jnp.concatenate([pv_ref[:, cols], v_ref[:, cols]], axis=0)
        d_out = do_ref[:, cols]
        bias = bias_blocks(table_ref[h : h + 1])
        dk = [None] * (blocks + WINDOW - 1)
        dv = [None] * (blocks + WINDOW - 1)
        d_band = [None] * WINDOW
        for p in range(blocks):
            at = slice(p * BLOCK, (p + 1) * BLOCK)
            window = slice(p * BLOCK, (p + WINDOW) * BLOCK)
            q_b, do_b, k_w, v_w = q_norm[at], d_out[at], k_norm[window], v_ext[window]
            here = [
                jnp.where(first, MASKED, b) if p + w < WINDOW - 1 else b for w, b in enumerate(bias)
            ]
            s = dot(k_w, q_b, (1, 1)) * FACTOR + jnp.concatenate(here, axis=0)
            e = jnp.exp(s - jnp.max(s, axis=0, keepdims=True))
            prob = e * (1.0 / jnp.sum(e, axis=0, keepdims=True))
            d_prob = dot(v_w, do_b, (1, 1))
            delta = jnp.sum(prob * d_prob, axis=0, keepdims=True)
            d_score = prob * (d_prob - delta)
            prob_low = prob.astype(BF16)
            d_low = d_score.astype(BF16)
            dv_w = dot(prob_low, do_b, (1, 0))
            dk_w = dot(d_low, q_b, (1, 0)) * FACTOR
            dq = dot(d_low, k_w, (0, 0)) * FACTOR
            for w in range(WINDOW):
                rng = slice(w * BLOCK, (w + 1) * BLOCK)
                dk[p + w] = dk_w[rng] if dk[p + w] is None else dk[p + w] + dk_w[rng]
                dv[p + w] = dv_w[rng] if dv[p + w] is None else dv[p + w] + dv_w[rng]
                d_band[w] = d_score[rng] if d_band[w] is None else d_band[w] + d_score[rng]
            d_gain_q = d_gain_q + jnp.sum(dq * q_unit[at], axis=0, keepdims=True)
            dq_ref[at, cols] = rows_back(dq, q_unit[at], q_rms[at], gain_q).astype(BF16)
        for b in range(blocks + WINDOW - 1):
            at = slice(b * BLOCK, (b + 1) * BLOCK)
            d_gain_k = d_gain_k + jnp.sum(dk[b] * k_unit[at], axis=0, keepdims=True)
            if b < WINDOW - 1:
                back_ref[b * BLOCK : (b + 1) * BLOCK, cols] = dk[b].astype(BF16)
                back_ref[TAIL + b * BLOCK : TAIL + (b + 1) * BLOCK, cols] = dv[b].astype(BF16)
            else:
                o = (b - WINDOW + 1) * BLOCK
                own_ref[o : o + BLOCK, cols] = dk[b]
                own_ref[rows + o : rows + o + BLOCK, cols] = dv[b]
        row = table_row(*d_band)
        pieces += [row[:, :HEAD_DIM], row[:, HEAD_DIM:]]
    pieces += [d_gain_q, d_gain_k]
    count = parts_ref.shape[1]
    pieces += [jnp.zeros((count - len(pieces), HEAD_DIM), F32)]
    parts_ref[...] = jnp.broadcast_to(jnp.concatenate(pieces, axis=0)[None], parts_ref.shape)


def final_kernel(k_ref, gains_ref, own_ref, back_ref, parts_ref, dk_ref, dv_ref, dt_ref, dg_ref):
    rows, features = k_ref.shape
    heads = features // HEAD_DIM
    sp, tp = lax.axis_size("sp"), lax.axis_size("tp")
    tail = slice(rows - TAIL, rows)
    for h in range(heads):
        cols = slice(h * HEAD_DIM, (h + 1) * HEAD_DIM)
        dk = own_ref[:rows, cols]
        dv = own_ref[rows:, cols]
        back_k = back_ref[:TAIL, cols].astype(F32)
        back_v = back_ref[TAIL:, cols].astype(F32)
        if rows > TAIL:
            zeros = jnp.zeros((rows - TAIL, HEAD_DIM), F32)
            back_k = jnp.concatenate([zeros, back_k], axis=0)
            back_v = jnp.concatenate([zeros, back_v], axis=0)
        k_unit, k_rms = unit_rows(k_ref[:, cols])
        dk_ref[:, cols] = rows_back(dk + back_k, k_unit, k_rms, gains_ref[1:2]).astype(BF16)
        dv_ref[:, cols] = (dv + back_v).astype(BF16)
    parts = parts_ref[...]
    parts = jnp.sum(parts.reshape(sp, tp, *parts.shape[1:]), axis=0)
    mine = parts[0]
    for i in range(1, tp):
        mine = jnp.where(lax.axis_index("tp") == i, parts[i], mine)
    for h in range(heads):
        row = jnp.concatenate([mine[2 * h : 2 * h + 1], mine[2 * h + 1 : 2 * h + 2]], axis=1)
        dt_ref[h : h + 1, :] = row[:, :ENTRIES]
    dg_ref[...] = jnp.sum(parts, axis=0)[2 * heads : 2 * heads + 2]


def local(queries, keys, values, gains, bias_table, d_out):
    rows, features = queries.shape
    heads = features // HEAD_DIM
    members = lax.axis_size("sp") * lax.axis_size("tp")
    count = -(-(2 * heads + 2) // 8) * 8
    prev_v = shifted(values[rows - TAIL :], 1)
    prev_k = shifted(keys[rows - TAIL :], 1)
    shape = jax.ShapeDtypeStruct
    d_queries, back, own, parts = pl.pallas_call(
        band_kernel,
        out_shape=(
            shape((rows, features), BF16),
            shape((2 * TAIL, features), BF16),
            shape((2 * rows, features), F32),
            shape((members, count, HEAD_DIM), F32),
        ),
        name="band",
    )(queries, keys, values, d_out, prev_k, prev_v, gains, bias_table.T)
    back = shifted(back, -1)
    parts = lax.all_to_all(parts, ("sp", "tp"), 0, 0)
    d_keys, d_values, d_table, d_gains = pl.pallas_call(
        final_kernel,
        out_shape=(
            shape((rows, features), BF16),
            shape((rows, features), BF16),
            shape((heads, ENTRIES), F32),
            shape((2, HEAD_DIM), F32),
        ),
        name="final",
    )(keys, gains, own, back, parts)
    return d_queries, d_keys, d_values, d_table.T, d_gains


def solution(mesh):
    in_specs = (P("sp", "tp"), P("sp", "tp"), P("sp", "tp"), P(), P(None, "tp"), P("sp", "tp"))
    out_specs = (P("sp", "tp"), P("sp", "tp"), P("sp", "tp"), P(None, "tp"), P())
    return jax.shard_map(local, mesh=mesh, in_specs=in_specs, out_specs=out_specs, check_vma=False)
```

time: 89.6 us -> 38.2 us (0.43)
  blocking collectives: 43.9 us -> 17.1 us
  local copies, waits for them, and re-layouts: 17.2 us -> 1.36 us
  other arithmetic: 7.59 us -> 0 us
  Pallas kernels: 0 us -> 6.44 us
  matrix products: 3.45 us -> 0 us
  starting transfers between devices: 11.3 us -> 9.56 us
  waiting for transfers between devices: 4.33 us -> 2.79 us
    psum x1 -> x0, blocking collectives: 43.9 us -> none  [local(): whole_table, d_gains = lax.psum((whole_table, gain_part), ('sp', 'tp'))]
    all_to_all x0 -> x1, blocking collectives: none -> 17.1 us  [local(): parts = lax.all_to_all(parts, ('sp', 'tp'), 0, 0)]
    pallas_call x0 -> x2, Pallas kernels: none -> 6.44 us  [the longest x1 4.28 us: local(): pl.pallas_call(band_kernel, out_shape=(shape((rows, features), BF16), sha...]
    reshape x7 -> x0, local copies, waits for them, and re-layouts: 4.92 us -> none  [the longest x2 3.38 us: unband(): pieces = grad_band.reshape(seg_count, LEFT + 1, SEG, -1)]
    mul x10 -> x0, local copies, waits for them, and re-layouts: 4.7 us -> none  [the longest x3 1.33 us: norm_rows(): unit_part * gain_vec]
    dot_general x5 -> x0, matrix products: 3.45 us -> none  [the longest x1 1.48 us: band_grads(): jnp.einsum('chij,cjhd->cihd', d_low, k_band, preferred_element_type=jnp.f...]
    reduce_sum x10 -> x0, other arithmetic: 3.4 us -> none  [the longest x1 0.77 us: table_grad(): tail_sum = jnp.sum(columns[:, entries - 1:], axis=1) + far_total]
    convert_element_type x4 -> x0, other arithmetic: 3.08 us -> none  [the longest x1 1.6 us: local(): d_values = dv_total.astype(jnp.bfloat16)]
  transfers between devices with their start and end apart: 4 -> 3, of which waited for: 1 -> 1; matrix products, arithmetic and copies ran while one was open for 13% -> 0% of each run, Pallas kernels for 0% -> 0%
where the time goes in v1:
time: 38.2 us; the launch traced here: 37.9 us
  blocking collectives  17.1 us (45%)
  starting transfers between devices  9.56 us (25%)
  Pallas kernels  6.44 us (17%)
  waiting for transfers between devices  2.79 us (7%)
  local copies, waits for them, and re-layouts  1.36 us (4%)
  between operations  0.68 us (2%)
    all_to_all x1, blocking collectives, local(): parts = lax.all_to_all(parts, ('sp', 'tp'), 0, 0)  17.1 us
    ppermute x3, starting transfers between devices, shifted(): return lax.ppermute(block, 'sp', route)  9.56 us
    pallas_call x1, Pallas kernels, local(): pl.pallas_call(band_kernel, out_shape=(shape((rows, features), BF16), sha...  4.28 us
    ppermute x3, waiting for transfers between devices, shifted(): return lax.ppermute(block, 'sp', route)  2.79 us
    pallas_call x1, Pallas kernels, local(): pl.pallas_call(final_kernel, out_shape=(shape((rows, features), BF16), sh...  2.17 us
    unnamed x6, local copies, waits for them, and re-layouts  1.36 us
  transfers between devices with their start and end apart: 3, of which 1 were waited for; matrix products, arithmetic and copies ran while one was open for 0% of the time, Pallas kernels for 0%

profile of v1, /device:TPU:0, one launch (start us, length us, event | category | flops | bytes accessed | tf_op | source)
XLA Modules:
  0.0 37.9 jit_solution(4965815358550415870)
XLA Ops:
  0.6 4.9 %collective-permute-start.1 = (bf16[256,256]{1,0:T(8,128)(2,1)}, bf16[256,256]{1,0:T(8,128)(2,1)S(1)}, u32[]{:S(2)}, u32[]{:S(2)}) collective-permute-start(bf16[256,256]{1,0:T(8,128)(2,1)} %v_ref.1), channel_id=1, source_target_pairs={{0,2},{2,4},{4,6},{6,8},{8,10},{10,12},{12,14},{14,16},{16,18},{18... | collective-permute-start | bytes 393224 | tf_op jit(solution)/shard_map/ppermute | solution.py:34
  5.5 3.4 %collective-permute-start = (bf16[256,256]{1,0:T(8,128)(2,1)}, bf16[256,256]{1,0:T(8,128)(2,1)S(1)}, u32[]{:S(2)}, u32[]{:S(2)}) collective-permute-start(bf16[256,256]{1,0:T(8,128)(2,1)} %k_ref.3), channel_id=1, source_target_pairs={{0,2},{2,4},{4,6},{6,8},{8,10},{10,12},{12,14},{14,16},{16,18},{18... | collective-permute-start | bytes 393224 | tf_op jit(solution)/shard_map/ppermute | solution.py:34
  8.9 0.0 collective-permute-done.1.pv_ref
  8.9 0.0 copy-start.1
  8.9 2.8 %collective-permute-done.pk_ref = bf16[256,256]{1,0:T(8,128)(2,1)S(1)} collective-permute-done((bf16[256,256]{1,0:T(8,128)(2,1)}, bf16[256,256]{1,0:T(8,128)(2,1)S(1)}, u32[]{:S(2)}, u32[]{:S(2)}) %collective-permute-start) | collective-permute-done | bytes 131104 | tf_op jit(solution)/shard_map/ppermute | solution.py:34
  11.7 0.0 copy-start.2
  11.7 0.0 copy-done.1
  11.7 0.7 %copy-done.2 = bf16[256,256]{1,0:T(8,128)(2,1)} copy-done((bf16[256,256]{1,0:T(8,128)(2,1)}, bf16[256,256]{1,0:T(8,128)(2,1)S(1)}, u32[]{:S(2)}) %copy-start.2) | copy-done | bytes 131096
  12.4 4.3 %band.1 = (bf16[256,256]{1,0:T(8,128)(2,1)}, bf16[512,256]{1,0:T(8,128)(2,1)}, f32[512,256]{1,0:T(8,128)}, f32[32,8,128]{2,1,0:T(8,128)}) custom-call(bf16[256,256]{1,0:T(8,128)(2,1)} %q_ref.1, bf16[256,256]{1,0:T(8,128)(2,1)} %k_ref.3, bf16[256,256]{1,0:T(8,128)(2,1)} %v_ref.1, bf16[256,256]{1,0:T(8,128)(2,1)} %do_ref.1, bf16[256,256]{1,0:T(8,128)(2,1)} %copy-done.2, ...), custom_call_target="tpu_custom_call" | custom-call | tf_op jit(solution)/shard_map/band/pallas_call | solution.py:203
  16.7 1.3 %collective-permute-start.2 = (bf16[512,256]{1,0:T(8,128)(2,1)}, bf16[512,256]{1,0:T(8,128)(2,1)S(1)}, u32[]{:S(2)}, u32[]{:S(2)}) collective-permute-start(bf16[512,256]{1,0:T(8,128)(2,1)} %get-tuple-element.15), channel_id=1, source_target_pairs={{2,0},{4,2},{6,4},{8,6},{10,8},{12,10},{14,12},{16,14},{18,16},{20... | collective-permute-start | bytes 786440 | tf_op jit(solution)/shard_map/ppermute | solution.py:34
  18.0 17.1 %all_to_all.5.parts_ref = f32[32,8,128]{2,1,0:T(8,128)} all-to-all(f32[32,8,128]{2,1,0:T(8,128)} %get-tuple-element.16), channel_id=1, replica_groups=mesh['sp'=16,'tp'=2] {'sp','tp'}, dimensions={0} | all-to-all | bytes 262144 | tf_op jit(solution)/shard_map/all_to_all | solution.py:214
  35.0 0.0 collective-permute-done.2.back_ref
  35.1 0.0 copy-start
  35.1 0.7 %copy-done = bf16[512,256]{1,0:T(8,128)(2,1)} copy-done((bf16[512,256]{1,0:T(8,128)(2,1)}, bf16[512,256]{1,0:T(8,128)(2,1)S(1)}, u32[]{:S(2)}) %copy-start) | copy-done | bytes 262168
  35.8 2.2 %final.1 = (bf16[256,256]{1,0:T(8,128)(2,1)}, bf16[256,256]{1,0:T(8,128)(2,1)}, f32[2,192]{1,0:T(2,128)}, f32[2,128]{1,0:T(2,128)}) custom-call(bf16[256,256]{1,0:T(8,128)(2,1)} %k_ref.3, f32[2,128]{1,0:T(2,128)} %gains_ref.3, f32[512,256]{1,0:T(8,128)} %get-tuple-element.14.own_ref, bf16[512,256]{1,0:T(8,128)(2,1)} %copy-done, ...), custom_call_target="tpu_custom_call" | custom-call | tf_op jit(solution)/shard_map/final/pallas_call | solution.py:215
Async XLA Ops:
  0.6 8.3 %collective-permute-start.1 = (bf16[256,256]{1,0:T(8,128)(2,1)}, bf16[256,256]{1,0:T(8,128)(2,1)S(1)}, u32[]{:S(2)}, u32[]{:S(2)}) collective-permute-start(bf16[256,256]{1,0:T(8,128)(2,1)} %v_ref.1), channel_id=1, source_target_pairs={{0,2},{2,4},{4,6},{6,8},{8,10},{10,12},{12,14},{14,16},{16,18},{18... | collective-permute-start | bytes 393224 | tf_op jit(solution)/shard_map/ppermute | solution.py:34
  5.5 6.2 %collective-permute-start = (bf16[256,256]{1,0:T(8,128)(2,1)}, bf16[256,256]{1,0:T(8,128)(2,1)S(1)}, u32[]{:S(2)}, u32[]{:S(2)}) collective-permute-start(bf16[256,256]{1,0:T(8,128)(2,1)} %k_ref.3), channel_id=1, source_target_pairs={{0,2},{2,4},{4,6},{6,8},{8,10},{10,12},{12,14},{14,16},{16,18},{18... | collective-permute-start | bytes 393224 | tf_op jit(solution)/shard_map/ppermute | solution.py:34
  8.9 2.8 %copy-start.1 = (bf16[256,256]{1,0:T(8,128)(2,1)}, bf16[256,256]{1,0:T(8,128)(2,1)S(1)}, u32[]{:S(2)}) copy-start(bf16[256,256]{1,0:T(8,128)(2,1)S(1)} %collective-permute-done.1.pv_ref) | copy-start | bytes 393220
  11.7 0.7 %copy-start.2 = (bf16[256,256]{1,0:T(8,128)(2,1)}, bf16[256,256]{1,0:T(8,128)(2,1)S(1)}, u32[]{:S(2)}) copy-start(bf16[256,256]{1,0:T(8,128)(2,1)S(1)} %collective-permute-done.pk_ref) | copy-start | bytes 393220
  16.7 18.4 %collective-permute-start.2 = (bf16[512,256]{1,0:T(8,128)(2,1)}, bf16[512,256]{1,0:T(8,128)(2,1)S(1)}, u32[]{:S(2)}, u32[]{:S(2)}) collective-permute-start(bf16[512,256]{1,0:T(8,128)(2,1)} %get-tuple-element.15), channel_id=1, source_target_pairs={{2,0},{4,2},{6,4},{8,6},{10,8},{12,10},{14,12},{16,14},{18,16},{20... | collective-permute-start | bytes 786440 | tf_op jit(solution)/shard_map/ppermute | solution.py:34
  35.1 0.7 %copy-start = (bf16[512,256]{1,0:T(8,128)(2,1)}, bf16[512,256]{1,0:T(8,128)(2,1)S(1)}, u32[]{:S(2)}) copy-start(bf16[512,256]{1,0:T(8,128)(2,1)S(1)} %collective-permute-done.2.back_ref) | copy-start | bytes 786436
